TPU v7x, 32 devices: a whole 2x2x4 slice. The times are simulated.
32 devices in a mesh: ep: 16 (over z, y, core), tp: 2 (over x).
Axes of the slice: x: 2, y: 2, z: 4, core: 2. Of those that a mesh axis runs over, the one named last changes fastest.
Arguments:
- tokens: bfloat16 [256, 2048], P('ep'), may hold values from -6 to 6
- positions: int32 [256], P('ep'), may hold values from 1024 to 16383
- state: float32 [256, 4, 128, 128], P('ep', 'tp'), may hold values from -1 to 1
- mix_gain: float32 [2048], replicated, may hold values from 0.1 to 1.9
- w_query: bfloat16 [2048, 512], P(None, 'tp'), may hold values from -0.125 to 0.125
- w_key: bfloat16 [2048, 512], P(None, 'tp'), may hold values from -0.125 to 0.125
- w_value: bfloat16 [2048, 512], P(None, 'tp'), may hold values from -0.125 to 0.125
- w_out: bfloat16 [512, 2048], P('tp'), may hold values from -0.25 to 0.25
- ffn_gain: float32 [2048], replicated, may hold values from 0.1 to 1.9
- branch_gate: bfloat16 [2048], replicated, may hold values from -0.125 to 0.125
- dense_gate: bfloat16 [2048, 4096], P('tp', 'ep'), may hold values from -0.125 to 0.125
- dense_up: bfloat16 [2048, 4096], P('tp', 'ep'), may hold values from -0.125 to 0.125
- dense_down: bfloat16 [4096, 2048], P('ep', 'tp'), may hold values from -0.09375 to 0.09375
- routes: int32 [256, 6], P('ep'), may hold values from 0 to 15, all different within a row; in each aligned block of 16 rows (0 to 15, 16 to 31, ...) at most 12 rows name the same one
- route_scores: float32 [256, 6], P('ep'), may hold values from 0.05 to 1
- expert_gate: bfloat16 [16, 2048, 512], P('ep', None, 'tp'), may hold values from -0.125 to 0.125
- expert_up: bfloat16 [16, 2048, 512], P('ep', None, 'tp'), may hold values from -0.125 to 0.125
- expert_down: bfloat16 [16, 512, 2048], P('ep', 'tp'), may hold values from -0.25 to 0.25
Outputs:
- layer_out: bfloat16 [256, 2048], P('ep', 'tp')
Inputs may be any that keep to these rules, and one draw needn't show every extreme that they name: `routes`: each row names 6 different experts. In each aligned block of 16 rows (the rows of one index of ep) no expert is named by more than 12 rows, a bound that some block reaches.
All inputs are finite; a program needn't handle non-finite values.
Results may differ from a plain program's by a relative error of at most 0.012.
Values may be sent and summed in bfloat16 or wider, within the bound.
A program may use at most 64 MiB of HBM per device.

v0:
```python
import jax
import jax.numpy as jnp
from jax import lax
from jax.sharding import PartitionSpec as P

EPS = 1e-06


def normalize(inputs, scale_vec):
    values = inputs.astype(jnp.float32)
    return values * lax.rsqrt(jnp.mean(values * values, axis=-1, keepdims=True) + EPS) * scale_vec


def rotate(vectors, where):
    half = vectors.shape[-1] // 2
    inverse = 1.0 / 10000.0 ** jnp.linspace(0.0, 1.0, half, dtype=jnp.float32)
    angle = where.astype(jnp.float32)[:, None] * inverse[None, :]
    cosine = jnp.cos(angle)[:, None, :]
    sine = jnp.sin(angle)[:, None, :]
    first = vectors[..., :half]
    second = vectors[..., half:]
    return jnp.concatenate(
        [first * cosine - second * sine, second * cosine + first * sine], axis=-1
    )


def on_device(
    tokens,
    positions,
    state,
    mix_gain,
    w_query,
    w_key,
    w_value,
    w_out,
    ffn_gain,
    branch_gate,
    dense_gate,
    dense_up,
    dense_down,
    routes,
    route_scores,
    expert_gate,
    expert_up,
    expert_down,
):
    sequences = tokens.shape[0]
    model_width = tokens.shape[1]
    tp_count = lax.axis_size("tp")
    ep_count = lax.axis_size("ep")
    columns = model_width // tp_count
    tp_index = lax.axis_index("tp")
    local_heads = state.shape[1]
    head_dim = state.shape[2]
    normed = normalize(tokens, mix_gain).astype(jnp.bfloat16)
    query_vec = jnp.dot(normed, w_query, preferred_element_type=jnp.float32).reshape(
        sequences, local_heads, head_dim
    )
    key_vec = jnp.dot(normed, w_key, preferred_element_type=jnp.float32).reshape(
        sequences, local_heads, head_dim
    )
    value_vec = jnp.dot(normed, w_value, preferred_element_type=jnp.float32).reshape(
        sequences, local_heads, head_dim
    )
    query_vec = rotate(query_vec, positions)
    key_vec = rotate(key_vec, positions) * head_dim ** (-0.5)
    all_heads = local_heads * tp_count
    head_index = (tp_index * local_heads + jnp.arange(local_heads, dtype=jnp.int32)).astype(
        jnp.float32
    )
    decay_rate = 1.0 - 2.0 ** (-5.0 - 5.0 * head_index / (all_heads - 1))
    new_state = (
        decay_rate[None, :, None, None] * state + key_vec[:, :, :, None] * value_vec[:, :, None, :]
    )
    retrieved = jnp.einsum("bhd,bhde->bhe", query_vec, new_state, precision=lax.Precision.HIGHEST)
    retrieved = retrieved * lax.rsqrt(jnp.mean(retrieved * retrieved, axis=-1, keepdims=True) + EPS)
    retrieved = retrieved.reshape(sequences, local_heads * head_dim).astype(jnp.bfloat16)
    head_partial = jnp.dot(retrieved, w_out, preferred_element_type=jnp.float32).astype(
        jnp.bfloat16
    )
    mixer_out = lax.psum(head_partial.astype(jnp.float32).astype(jnp.bfloat16), "tp").astype(
        jnp.float32
    )
    after_mix = tokens.astype(jnp.float32) + mixer_out
    ffn_in = normalize(after_mix, ffn_gain).astype(jnp.bfloat16)
    own_cols = lax.dynamic_slice_in_dim(ffn_in, tp_index * columns, columns, 1)
    per_device = expert_gate.shape[0]
    experts = per_device * ep_count
    fanout = routes.shape[1]
    capacity = max(2, min(sequences, 2 * sequences * fanout // experts))
    slot_count = experts * capacity
    marks = (routes[:, :, None] == jnp.arange(experts, dtype=jnp.int32)[None, None, :]).astype(
        jnp.int32
    )
    flattened = marks.reshape(sequences * fanout, experts)
    ranking = jnp.sum((jnp.cumsum(flattened, axis=0) - flattened) * flattened, axis=1).reshape(
        sequences, fanout
    )
    slot_index = routes * capacity + ranking
    matches = jnp.arange(slot_count, dtype=jnp.int32)[:, None, None] == slot_index[None]
    placing = jnp.any(matches, axis=2).astype(jnp.bfloat16)
    route_weights = route_scores / jnp.sum(route_scores, axis=1, keepdims=True)
    combining = jnp.sum(jnp.where(matches, route_weights[None], 0.0), axis=2).T
    packed = jnp.dot(placing, own_cols, preferred_element_type=jnp.float32).astype(jnp.bfloat16)
    packed = packed.reshape(experts, capacity, own_cols.shape[1])
    received = lax.all_to_all(packed, "ep", split_axis=0, concat_axis=0, tiled=True)
    received = lax.all_gather(received, "tp", axis=2, tiled=True)
    count = received.shape[1]
    grouped = received.reshape(ep_count, per_device, count, model_width)
    gate_pre = jnp.einsum(
        "skcd,kdw->skcw", grouped, expert_gate, preferred_element_type=jnp.float32
    )
    up_pre = jnp.einsum("skcd,kdw->skcw", grouped, expert_up, preferred_element_type=jnp.float32)
    hidden = (jax.nn.silu(gate_pre) * up_pre).astype(jnp.bfloat16)
    partial_out = jnp.einsum(
        "skcw,kwd->skcd", hidden, expert_down, preferred_element_type=jnp.float32
    )
    blocks_out = partial_out.astype(jnp.bfloat16).reshape(
        ep_count, per_device, count, tp_count, columns
    )
    traded = lax.all_to_all(blocks_out, "tp", split_axis=3, concat_axis=3, tiled=True)
    mine = jnp.sum(traded.astype(jnp.float32), axis=3).astype(jnp.bfloat16)
    mine = mine.reshape(ep_count * per_device, count, columns)
    returned = lax.all_to_all(mine, "ep", split_axis=0, concat_axis=0, tiled=True)
    experts_out = jnp.dot(
        combining,
        returned.reshape(slot_count, columns).astype(jnp.float32),
        precision=lax.Precision.HIGHEST,
    )
    hidden_units = dense_gate.shape[1]
    both_weights = jnp.concatenate([dense_gate, dense_up], axis=1)
    pre_parts = jnp.dot(
        lax.all_gather(own_cols, "ep", axis=0, tiled=True),
        both_weights,
        preferred_element_type=jnp.float32,
    ).astype(jnp.bfloat16)
    pre_total = lax.psum(pre_parts.astype(jnp.float32).astype(jnp.bfloat16), "tp").astype(
        jnp.float32
    )
    dense_hidden = (jax.nn.silu(pre_total[:, :hidden_units]) * pre_total[:, hidden_units:]).astype(
        jnp.bfloat16
    )
    dense_out = lax.psum_scatter(
        jnp.dot(dense_hidden, dense_down, preferred_element_type=jnp.float32),
        "ep",
        scatter_dimension=0,
        tiled=True,
    )
    branch_weight = jax.nn.sigmoid(jnp.dot(ffn_in, branch_gate, preferred_element_type=jnp.float32))
    residual_cols = lax.dynamic_slice_in_dim(after_mix, tp_index * columns, columns, 1)
    layer_out = residual_cols + experts_out + branch_weight[:, None] * dense_out
    return layer_out.astype(jnp.bfloat16)


def solution(mesh):
    placed = (
        P("ep", None),
        P("ep"),
        P("ep", "tp", None, None),
        P(),
        P(None, "tp"),
        P(None, "tp"),
        P(None, "tp"),
        P("tp", None),
        P(),
        P(),
        P("tp", "ep"),
        P("tp", "ep"),
        P("ep", "tp"),
        P("ep", None),
        P("ep", None),
        P("ep", None, "tp"),
        P("ep", None, "tp"),
        P("ep", "tp", None),
    )
    return jax.shard_map(
        on_device, mesh=mesh, in_specs=placed, out_specs=P("ep", "tp"), check_vma=False
    )
```

profile of v0, /device:TPU:0, one launch (start us, length us, event | category | flops | bytes accessed | tf_op | source)
XLA Modules:
  0.0 169.2 jit_solution(17816289287856958037)
XLA Ops:
  6.6 0.8 convert_element_type.77
  7.4 1.0 fusion.30
  8.5 1.6 fusion.47
  10.1 1.6 fusion.45
  11.7 1.5 fusion.49
  13.7 2.1 %fusion = f32[16,2,1,128]{3,2,1,0:T(1,128)S(1)} fusion(f32[16,2,128,1]{2,3,1,0:T(1,128)S(1)} %bitcast.86, f32[16,2,128,128]{3,2,1,0:T(8,128)S(1)} %copy-done.2, f32[16,2,128]{2,1,0:T(2,128)S(1)} %mul.244, f32[16,2,128]{2,1,0:T(2,128)S(1)} %get-tuple-element.17, f32[2]{0:T(128)S(1)} %power_subtract_fusion), kind=kOutput, calls=%fused_computation.2 | convolution fusion | flops 7864320 | bytes 2162696 | tf_op jit(solution)/shard_map/bhd,bhde->bhe/dot_general | solution.py:75
  15.9 0.9 convolution_convert_fusion.1
  17.1 0.1 reduce_window_sum.11
  17.3 0.2 select_reduce_fusion.1
  17.7 23.0 %all-reduce.3.cloned.1.call-done = bf16[16,2048]{1,0:T(8,128)(2,1)} async-done(((bf16[16,2048]{1,0:T(8,128)(2,1)}), bf16[16,2048]{1,0:T(8,128)(2,1)}) %all-reduce.3.cloned.1.call-update) | async-done | bytes 65552 | tf_op jit(solution)/shard_map/psum | solution.py:81
  40.7 1.6 convert_add_fusion
  42.3 0.9 multiply_convert_fusion
  43.3 22.9 %all_gather.7 = bf16[256,1024]{1,0:T(8,128)(2,1)S(1)} all-gather(bf16[16,1024]{1,0:T(8,128)(2,1)S(1)} %constant_dynamic-slice_fusion), channel_id=1, replica_groups=mesh['ep'=16,'tp'=2] {'ep'}, dimensions={0}, use_global_device_ids=true | all-gather | bytes 557056 | tf_op jit(solution)/shard_map/all_gather | solution.py:133
  66.2 0.3 convolution_convert_fusion.2
  66.5 0.9 reshape.155
  67.4 3.6 %all-to-all-start = ((bf16[16,12,1024]{2,1,0:T(8,128)(2,1)}), bf16[16,12,1024]{2,1,0:T(8,128)(2,1)S(1)}, u32[]{:S(2)}, u32[]{:S(2)}) async-start(bf16[16,12,1024]{2,1,0:T(8,128)(2,1)} %reshape.155), calls=%async_computation | async-start | bytes 1048576 | tf_op jit(solution)/shard_map/all_to_all | solution.py:106
  71.0 2.2 %convolution_convert_fusion.3 = bf16[256,512]{1,0:T(8,128)(2,1)} fusion(bf16[256,1024]{1,0:T(8,128)(2,1)S(1)} %all_gather.7, bf16[1024,256]{1,0:T(8,128)(2,1)S(1)} %copy-done.12, bf16[1024,256]{1,0:T(8,128)(2,1)} %param.30), kind=kOutput, calls=%fused_computation.7 | convolution fusion | flops 270663680 | bytes 1835008 | tf_op jit(solution)/shard_map/dot_general | solution.py:132
  73.3 24.4 %all-reduce.5.cloned.1.call-done = bf16[256,512]{1,0:T(8,128)(2,1)} async-done(((bf16[256,512]{1,0:T(8,128)(2,1)}), bf16[256,512]{1,0:T(8,128)(2,1)}) %all-reduce.5.cloned.1.call-update) | async-done | bytes 262160 | tf_op jit(solution)/shard_map/psum | solution.py:137
  97.7 1.0 convert_element_type.92
  98.8 1.3 fusion.33
  100.1 0.2 copy.61
  100.3 11.0 %all_gather.6 = bf16[16,12,2048]{2,0,1:T(8,128)(2,1)S(1)} all-gather(bf16[16,12,1024]{2,0,1:T(8,128)(2,1)S(1)} %copy.61), channel_id=1, replica_groups=mesh['ep'=16,'tp'=2] {'tp'}, dimensions={2}, use_global_device_ids=true | all-gather | bytes 1179648 | tf_op jit(solution)/shard_map/all_gather | solution.py:107
  111.4 1.1 convolution_bitcast_fusion.1
  112.4 2.3 %convolution_convert_fusion = bf16[16,12,2048]{2,0,1:T(8,128)(2,1)S(1)} fusion(bf16[1,256,2048]{2,1,0:T(8,128)(2,1)S(1)} %copy-done, bf16[16,12,2048]{2,0,1:T(8,128)(2,1)S(1)} %all_gather.6, bf16[1,2048,256]{2,1,0:T(8,128)(2,1)} %param.36, f32[16,1,12,256]{3,0,2,1:T(8,128)} %convolution_bitcast_fusion.1), kind=kOutput, calls=%fused_computation | convolution fusion | flops 403341312 | bytes 3866624 | tf_op jit(solution)/shard_map/skcw,kwd->skcd/dot_general | solution.py:115
  114.8 12.1 %all_to_all.15 = bf16[16,1,12,2,1024]{4,0,2,1,3:T(8,128)(2,1)S(1)} all-to-all(bf16[16,1,12,2,1024]{4,0,2,1,3:T(8,128)(2,1)S(1)} %bitcast.82), channel_id=1, replica_groups=mesh['ep'=16,'tp'=2] {'tp'}, dimensions={3} | all-to-all | bytes 1572864 | tf_op jit(solution)/shard_map/all_to_all | solution.py:121
  126.9 0.2 reduce_sum.72
  127.1 1.0 copy.64
  128.2 5.6 %all-to-all-start.2 = ((bf16[16,12,1024]{2,1,0:T(8,128)(2,1)}), bf16[16,12,1024]{2,1,0:T(8,128)(2,1)S(1)}, u32[]{:S(2)}, u32[]{:S(2)}) async-start(bf16[16,12,1024]{2,1,0:T(8,128)(2,1)} %copy.64), calls=%async_computation.2 | async-start | bytes 1048576 | tf_op jit(solution)/shard_map/all_to_all | solution.py:124
  134.0 0.1 fusion.12
  134.1 14.8 %all-to-all-done.2 = bf16[16,12,1024]{2,1,0:T(8,128)(2,1)S(1)} async-done(((bf16[16,12,1024]{2,1,0:T(8,128)(2,1)}), bf16[16,12,1024]{2,1,0:T(8,128)(2,1)S(1)}, u32[]{:S(2)}, u32[]{:S(2)}) %all-to-all-start.2) | async-done | bytes 393248 | tf_op jit(solution)/shard_map/all_to_all | solution.py:124
  149.0 11.9 %reduce-scatter.2.cloned.1.call-done = f32[16,1024]{1,0:T(8,128)} async-done(((f32[256,1024]{1,0:T(8,128)}), f32[16,1024]{1,0:T(8,128)}) %reduce-scatter.2.cloned.1.call-update) | async-done | bytes 65552 | tf_op jit(solution)/shard_map/reduce_scatter | solution.py:143
  160.9 1.7 %fusion.8 = bf16[16,1024]{1,0:T(8,128)(2,1)} fusion(f32[192,16]{0,1:T(8,128)S(1)} %select_reduce_fusion, bf16[192,1024]{1,0:T(8,128)(2,1)S(1)} %reshape.161, f32[16,1024]{1,0:T(8,128)} %reduce-scatter.2.cloned.1.call-done, f32[16,2048]{1,0:T(8,128)S(1)} %copy-done.6, s32[]{:T(128)S(6)} %select_n.8, f32[16]{0:T(128)S(1)} %fusion.12), kind=kOutput, calls=%fused_computation.15 | convolution fusion | flops 37814272 | bytes 569412 | tf_op jit(solution)/shard_map/dot_general | solution.py:125
  (61 shorter events, 1.7 us)
Async XLA Ops:
  6.5 105.9 %copy-start = (bf16[1,256,2048]{2,1,0:T(8,128)(2,1)S(1)}, bf16[1,256,2048]{2,1,0:T(8,128)(2,1)}, u32[]{:S(2)}) copy-start(bf16[1,256,2048]{2,1,0:T(8,128)(2,1)} %param.37) | copy-start | bytes 3145732
  6.5 5.1 %copy-start.1 = (bf16[16,2048]{1,0:T(8,128)(2,1)S(1)}, bf16[16,2048]{1,0:T(8,128)(2,1)}, u32[]{:S(2)}) copy-start(bf16[16,2048]{1,0:T(8,128)(2,1)} %param.20) | copy-start | bytes 196612
  6.5 5.1 %copy-start.7 = (f32[2048]{0:T(1024)S(1)}, f32[2048]{0:T(1024)}, u32[]{:S(2)}) copy-start(f32[2048]{0:T(1024)} %param.23) | copy-start | bytes 24580
  6.5 7.1 %copy-start.2 = (f32[16,2,128,128]{3,2,1,0:T(8,128)S(1)}, f32[16,2,128,128]{3,2,1,0:T(8,128)}, u32[]{:S(2)}) copy-start(f32[16,2,128,128]{3,2,1,0:T(8,128)} %param.22) | copy-start | bytes 6291460
  6.5 34.1 %all-reduce.3.cloned.1.call-start = ((), (), s32[]{:S(2)}) async-start(), calls=%async_computation.4 | async-start | bytes 131072 | tf_op jit(solution)/shard_map/psum | solution.py:81
  13.2 3.7 %copy-start.8 = (s32[16,6]{0,1:T(8,128)S(1)}, s32[16,6]{0,1:T(8,128)}, u32[]{:S(2)}) copy-start(s32[16,6]{0,1:T(8,128)} %param.33) | copy-start | bytes 1156
  13.2 2.7 %copy-start.3 = (bf16[256,2048]{1,0:T(8,128)(2,1)S(1)}, bf16[256,2048]{1,0:T(8,128)(2,1)}, u32[]{:S(2)}) copy-start(bf16[256,2048]{1,0:T(8,128)(2,1)} %param.27) | copy-start | bytes 3145732
  13.4 28.9 %copy-start.10 = (f32[2048]{0:T(1024)S(1)}, f32[2048]{0:T(1024)}, u32[]{:S(2)}) copy-start(f32[2048]{0:T(1024)} %param.28) | copy-start | bytes 24580
  16.8 54.2 %copy-start.12 = (bf16[1024,256]{1,0:T(8,128)(2,1)S(1)}, bf16[1024,256]{1,0:T(8,128)(2,1)}, u32[]{:S(2)}) copy-start(bf16[1024,256]{1,0:T(8,128)(2,1)} %param.31) | copy-start | bytes 1572868
  67.4 32.7 %all-to-all-start = ((bf16[16,12,1024]{2,1,0:T(8,128)(2,1)}), bf16[16,12,1024]{2,1,0:T(8,128)(2,1)S(1)}, u32[]{:S(2)}, u32[]{:S(2)}) async-start(bf16[16,12,1024]{2,1,0:T(8,128)(2,1)} %reshape.155), calls=%async_computation | async-start | bytes 1048576 | tf_op jit(solution)/shard_map/all_to_all | solution.py:106
  70.9 27.8 %copy-start.5 = (bf16[256,1024]{1,0:T(8,128)(2,1)S(1)}, bf16[256,1024]{1,0:T(8,128)(2,1)}, u32[]{:S(2)}) copy-start(bf16[256,1024]{1,0:T(8,128)(2,1)} %param.32) | copy-start | bytes 1572868
  71.0 26.8 %all-reduce.5.cloned.1.call-start = ((), (), s32[]{:S(2)}) async-start(), calls=%async_computation.5 | async-start | bytes 524288 | tf_op jit(solution)/shard_map/psum | solution.py:137
  73.3 87.6 %reduce-scatter.2.cloned.1.call-start = ((), (), s32[]{:S(2)}) async-start(), calls=%async_computation.6 | async-start | bytes 1114112 | tf_op jit(solution)/shard_map/reduce_scatter | solution.py:143
  98.8 12.6 %copy-start.4 = (bf16[1,2048,256]{2,1,0:T(8,128)(2,1)S(1)}, bf16[1,2048,256]{2,1,0:T(8,128)(2,1)}, u32[]{:S(2)}) copy-start(bf16[1,2048,256]{2,1,0:T(8,128)(2,1)} %param.35) | copy-start | bytes 3145732
  114.8 19.0 %copy-start.11 = (bf16[2048]{0:T(1024)(128)(2,1)S(1)}, bf16[2048]{0:T(1024)(128)(2,1)}, u32[]{:S(2)}) copy-start(bf16[2048]{0:T(1024)(128)(2,1)} %param.29) | copy-start | bytes 12292
  114.8 19.0 %copy-start.9 = (f32[16,6]{0,1:T(8,128)S(1)}, f32[16,6]{0,1:T(8,128)}, u32[]{:S(2)}) copy-start(f32[16,6]{0,1:T(8,128)} %param.34) | copy-start | bytes 1156
  126.9 34.0 %copy-start.6 = (f32[16,2048]{1,0:T(8,128)S(1)}, f32[16,2048]{1,0:T(8,128)}, u32[]{:S(2)}) copy-start(f32[16,2048]{1,0:T(8,128)} %get-tuple-element.6) | copy-start | bytes 393220
  128.2 20.7 %all-to-all-start.2 = ((bf16[16,12,1024]{2,1,0:T(8,128)(2,1)}), bf16[16,12,1024]{2,1,0:T(8,128)(2,1)S(1)}, u32[]{:S(2)}, u32[]{:S(2)}) async-start(bf16[16,12,1024]{2,1,0:T(8,128)(2,1)} %copy.64), calls=%async_computation.2 | async-start | bytes 1048576 | tf_op jit(solution)/shard_map/all_to_all | solution.py:124
Sparse Core Ops, SparseCore 0:
  17.0 23.6 all-reduce.2
  74.0 23.6 all-reduce.4
  101.4 59.4 reduce-scatter.1
where the time goes:
time: 170 us; the launch traced here: 169 us
  waiting for transfers between devices  74.1 us (44%)
  blocking collectives  46 us (27%)
  matrix products  16.6 us (10%)
  between operations  13.5 us (8%)
  starting transfers between devices  9.31 us (5%)
  other arithmetic  6.78 us (4%)
  local copies, waits for them, and re-layouts  2.79 us (2%)
    psum x1, waiting for transfers between devices, on_device(): lax.psum(pre_parts.astype(jnp.float32).astype(jnp.bfloat16), 'tp')  24.4 us
    psum x1, waiting for transfers between devices, on_device(): lax.psum(head_partial.astype(jnp.float32).astype(jnp.bfloat16), 'tp')  23 us
    all_gather x1, blocking collectives, on_device(): lax.all_gather(own_cols, 'ep', axis=0, tiled=True)  22.9 us
    all_to_all x1, waiting for transfers between devices, on_device(): lax.all_to_all(mine, 'ep', split_axis=0, concat_axis=0, tiled=True)  14.8 us
    all_to_all x1, blocking collectives, on_device(): lax.all_to_all(blocks_out, 'tp', split_axis=3, concat_axis=3, tiled=True)  12.1 us
    reduce_scatter x1, waiting for transfers between devices, on_device(): lax.psum_scatter(jnp.dot(dense_hidden, dense_down, preferred_element_type...  11.9 us
    all_gather x1, blocking collectives, on_device(): received = lax.all_gather(received, 'tp', axis=2, tiled=True)  11 us
    all_to_all x1, starting transfers between devices, on_device(): lax.all_to_all(mine, 'ep', split_axis=0, concat_axis=0, tiled=True)  5.62 us
  transfers between devices with their start and end apart: 5, of which 4 were waited for; matrix products, arithmetic and copies ran while one was open for 6% of the time, Pallas kernels for 0%

commit v1 on v0

--- a/solution.py
+++ b/solution.py
@@ -78,9 +78,9 @@
     head_partial = jnp.dot(retrieved, w_out, preferred_element_type=jnp.float32).astype(
         jnp.bfloat16
     )
-    mixer_out = lax.psum(head_partial.astype(jnp.float32).astype(jnp.bfloat16), "tp").astype(
-        jnp.float32
-    )
+    mixer_out = jnp.sum(
+        lax.all_gather(head_partial.astype(jnp.float32).astype(jnp.bfloat16), "tp"), axis=0
+    ).astype(jnp.float32)
     after_mix = tokens.astype(jnp.float32) + mixer_out
     ffn_in = normalize(after_mix, ffn_gain).astype(jnp.bfloat16)
     own_cols = lax.dynamic_slice_in_dim(ffn_in, tp_index * columns, columns, 1)

time: 170 us -> 158 us (0.929)
  waiting for transfers between devices: 74.1 us -> 50.1 us
  blocking collectives: 46 us -> 56 us
  starting transfers between devices: 9.31 us -> 12.2 us
    psum x1 -> x0, waiting for transfers between devices: 23 us -> none  [on_device(): lax.psum(head_partial.astype(jnp.float32).astype(jnp.bfloat16), 'tp')]
    all_gather x0 -> x1, blocking collectives: none -> 5.99 us  [on_device(): lax.all_gather(head_partial.astype(jnp.float32).astype(jnp.bfloat16), 'tp')]
    all_gather x1, blocking collectives: 22.9 us -> 26.8 us  [on_device(): lax.all_gather(own_cols, 'ep', axis=0, tiled=True)]
    all_to_all x1, starting transfers between devices: 3.57 us -> 6.48 us  [on_device(): lax.all_to_all(packed, 'ep', split_axis=0, concat_axis=0, tiled=True)]
    psum x1, waiting for transfers between devices: 24.4 us -> 21.8 us  [on_device(): lax.psum(pre_parts.astype(jnp.float32).astype(jnp.bfloat16), 'tp')]
  transfers between devices with their start and end apart: 5 -> 4, of which waited for: 4 -> 3; matrix products, arithmetic and copies ran while one was open for 6% -> 6% of each run, Pallas kernels for 0% -> 0%
where the time goes in v1:
time: 158 us; the launch traced here: 157 us
  blocking collectives  56 us (35%)
  waiting for transfers between devices  50.1 us (32%)
  matrix products  16.5 us (10%)
  between operations  13.7 us (9%)
  starting transfers between devices  12.2 us (8%)
  other arithmetic  5.13 us (3%)
  local copies, waits for them, and re-layouts  3.48 us (2%)
    all_gather x1, blocking collectives, on_device(): lax.all_gather(own_cols, 'ep', axis=0, tiled=True)  26.8 us
    psum x1, waiting for transfers between devices, on_device(): lax.psum(pre_parts.astype(jnp.float32).astype(jnp.bfloat16), 'tp')  21.8 us
    all_to_all x1, waiting for transfers between devices, on_device(): lax.all_to_all(mine, 'ep', split_axis=0, concat_axis=0, tiled=True)  15.2 us
    reduce_scatter x1, waiting for transfers between devices, on_device(): lax.psum_scatter(jnp.dot(dense_hidden, dense_down, preferred_element_type...  13 us
    all_to_all x1, blocking collectives, on_device(): lax.all_to_all(blocks_out, 'tp', split_axis=3, concat_axis=3, tiled=True)  12.1 us
    all_gather x1, blocking collectives, on_device(): received = lax.all_gather(received, 'tp', axis=2, tiled=True)  11 us
    all_to_all x1, starting transfers between devices, on_device(): lax.all_to_all(packed, 'ep', split_axis=0, concat_axis=0, tiled=True)  6.48 us
    all_gather x1, blocking collectives, on_device(): lax.all_gather(head_partial.astype(jnp.float32).astype(jnp.bfloat16), 'tp')  5.99 us
  transfers between devices with their start and end apart: 4, of which 3 were waited for; matrix products, arithmetic and copies ran while one was open for 6% of the time, Pallas kernels for 0%

profile of v1, /device:TPU:0, one launch (start us, length us, event | category | flops | bytes accessed | tf_op | source)
XLA Modules:
  0.0 157.1 jit_solution(18438197014540999177)
XLA Ops:
  6.6 0.8 convert_element_type.79
  7.4 1.0 fusion.30
  8.4 0.8 copy.59
  9.3 1.6 fusion.47
  10.9 1.6 fusion.45
  12.5 1.5 fusion.49
  14.5 2.1 %fusion = f32[16,2,1,128]{3,2,1,0:T(1,128)S(1)} fusion(f32[16,2,128,1]{2,3,1,0:T(1,128)S(1)} %bitcast.88, f32[16,2,128,128]{3,2,1,0:T(8,128)S(1)} %copy-done.2, f32[16,2,128]{2,1,0:T(2,128)S(1)} %mul.244, f32[16,2,128]{2,1,0:T(2,128)S(1)} %get-tuple-element.17, f32[2]{0:T(128)S(1)} %power_subtract_fusion), kind=kOutput, calls=%fused_computation.2 | convolution fusion | flops 7864320 | bytes 2162696 | tf_op jit(solution)/shard_map/bhd,bhde->bhe/dot_general | solution.py:75
  16.8 0.1 reduce_window_sum.11
  17.0 0.2 select_reduce_fusion.1
  17.4 1.5 convolution_convert_fusion.1
  18.9 6.0 %all-gather = bf16[32,2048]{1,0:T(8,128)(2,1)S(1)} all-gather(bf16[16,2048]{1,0:T(8,128)(2,1)S(1)} %convolution_convert_fusion.1), channel_id=2, replica_groups=mesh['ep'=16,'tp'=2] {'tp'}, dimensions={0}, use_global_device_ids=true | all-gather | bytes 196608 | tf_op jit(solution)/shard_map/all_gather | solution.py:82
  24.9 0.8 convert_add_fusion
  25.8 0.3 convolution_convert_fusion.2
  26.1 0.9 reshape.155
  27.0 6.5 %all-to-all-start = ((bf16[16,12,1024]{2,1,0:T(8,128)(2,1)}), bf16[16,12,1024]{2,1,0:T(8,128)(2,1)S(1)}, u32[]{:S(2)}, u32[]{:S(2)}) async-start(bf16[16,12,1024]{2,1,0:T(8,128)(2,1)} %reshape.155), calls=%async_computation | async-start | bytes 1048576 | tf_op jit(solution)/shard_map/all_to_all | solution.py:106
  33.6 26.8 %all_gather.15 = bf16[256,1024]{1,0:T(8,128)(2,1)S(1)} all-gather(bf16[16,1024]{1,0:T(8,128)(2,1)S(1)} %constant_dynamic-slice_fusion), channel_id=1, replica_groups=mesh['ep'=16,'tp'=2] {'ep'}, dimensions={0}, use_global_device_ids=true | all-gather | bytes 557056 | tf_op jit(solution)/shard_map/all_gather | solution.py:133
  60.4 2.2 %convolution_convert_fusion.3 = bf16[256,512]{1,0:T(8,128)(2,1)} fusion(bf16[256,1024]{1,0:T(8,128)(2,1)S(1)} %all_gather.15, bf16[1024,256]{1,0:T(8,128)(2,1)S(1)} %copy-done.11, bf16[1024,256]{1,0:T(8,128)(2,1)} %param.30), kind=kOutput, calls=%fused_computation.7 | convolution fusion | flops 270663680 | bytes 1835008 | tf_op jit(solution)/shard_map/dot_general | solution.py:132
  62.7 21.8 %all-reduce.2.cloned.1.call-done = bf16[256,512]{1,0:T(8,128)(2,1)} async-done(((bf16[256,512]{1,0:T(8,128)(2,1)}), bf16[256,512]{1,0:T(8,128)(2,1)}) %all-reduce.2.cloned.1.call-update) | async-done | bytes 262160 | tf_op jit(solution)/shard_map/psum | solution.py:137
  84.5 1.0 convert_element_type.94
  85.5 1.3 fusion.33
  86.9 0.2 copy.61
  87.1 11.0 %all_gather.14 = bf16[16,12,2048]{2,0,1:T(8,128)(2,1)S(1)} all-gather(bf16[16,12,1024]{2,0,1:T(8,128)(2,1)S(1)} %copy.61), channel_id=1, replica_groups=mesh['ep'=16,'tp'=2] {'tp'}, dimensions={2}, use_global_device_ids=true | all-gather | bytes 1179648 | tf_op jit(solution)/shard_map/all_gather | solution.py:107
  98.1 0.4 convolution_bitcast_fusion.1
  98.5 2.3 %convolution_convert_fusion = bf16[16,12,2048]{2,0,1:T(8,128)(2,1)S(1)} fusion(bf16[1,256,2048]{2,1,0:T(8,128)(2,1)S(1)} %copy-done, bf16[16,12,2048]{2,0,1:T(8,128)(2,1)S(1)} %all_gather.14, bf16[1,2048,256]{2,1,0:T(8,128)(2,1)} %param.36, f32[16,1,12,256]{3,0,2,1:T(8,128)S(1)} %convolution_bitcast_fusion.1), kind=kOutput, calls=%fused_computation | convolution fusion | flops 403341312 | bytes 3866624 | tf_op jit(solution)/shard_map/skcw,kwd->skcd/dot_general | solution.py:115
  100.9 12.1 %all_to_all.15 = bf16[16,1,12,2,1024]{4,0,2,1,3:T(8,128)(2,1)S(1)} all-to-all(bf16[16,1,12,2,1024]{4,0,2,1,3:T(8,128)(2,1)S(1)} %bitcast.83), channel_id=1, replica_groups=mesh['ep'=16,'tp'=2] {'tp'}, dimensions={3} | all-to-all | bytes 1572864 | tf_op jit(solution)/shard_map/all_to_all | solution.py:121
  113.0 0.2 reduce_sum.85
  113.2 1.0 copy.64
  114.2 5.6 %all-to-all-start.2 = ((bf16[16,12,1024]{2,1,0:T(8,128)(2,1)}), bf16[16,12,1024]{2,1,0:T(8,128)(2,1)S(1)}, u32[]{:S(2)}, u32[]{:S(2)}) async-start(bf16[16,12,1024]{2,1,0:T(8,128)(2,1)} %copy.64), calls=%async_computation.2 | async-start | bytes 1048576 | tf_op jit(solution)/shard_map/all_to_all | solution.py:124
  120.0 0.1 fusion.12
  120.2 15.2 %all-to-all-done.2 = bf16[16,12,1024]{2,1,0:T(8,128)(2,1)S(1)} async-done(((bf16[16,12,1024]{2,1,0:T(8,128)(2,1)}), bf16[16,12,1024]{2,1,0:T(8,128)(2,1)S(1)}, u32[]{:S(2)}, u32[]{:S(2)}) %all-to-all-start.2) | async-done | bytes 393248 | tf_op jit(solution)/shard_map/all_to_all | solution.py:124
  135.4 13.0 %reduce-scatter.2.cloned.1.call-done = f32[16,1024]{1,0:T(8,128)} async-done(((f32[256,1024]{1,0:T(8,128)}), f32[16,1024]{1,0:T(8,128)}) %reduce-scatter.2.cloned.1.call-update) | async-done | bytes 65552 | tf_op jit(solution)/shard_map/reduce_scatter | solution.py:143
  148.5 1.7 %fusion.8 = bf16[16,1024]{1,0:T(8,128)(2,1)} fusion(f32[192,16]{0,1:T(8,128)S(1)} %select_reduce_fusion, bf16[192,1024]{1,0:T(8,128)(2,1)S(1)} %reshape.161, f32[16,1024]{1,0:T(8,128)} %reduce-scatter.2.cloned.1.call-done, f32[16,2048]{1,0:T(8,128)S(1)} %copy-done.5, s32[]{:T(128)S(6)} %select_n.8, f32[16]{0:T(128)S(1)} %fusion.12), kind=kOutput, calls=%fused_computation.15 | convolution fusion | flops 37814272 | bytes 569412 | tf_op jit(solution)/shard_map/dot_general | solution.py:125
  (58 shorter events, 1.7 us)
Async XLA Ops:
  6.5 92.0 %copy-start = (bf16[1,256,2048]{2,1,0:T(8,128)(2,1)S(1)}, bf16[1,256,2048]{2,1,0:T(8,128)(2,1)}, u32[]{:S(2)}) copy-start(bf16[1,256,2048]{2,1,0:T(8,128)(2,1)} %param.37) | copy-start | bytes 3145732
  6.5 5.9 %copy-start.1 = (bf16[16,2048]{1,0:T(8,128)(2,1)S(1)}, bf16[16,2048]{1,0:T(8,128)(2,1)}, u32[]{:S(2)}) copy-start(bf16[16,2048]{1,0:T(8,128)(2,1)} %param.20) | copy-start | bytes 196612
  6.5 5.9 %copy-start.6 = (f32[2048]{0:T(1024)S(1)}, f32[2048]{0:T(1024)}, u32[]{:S(2)}) copy-start(f32[2048]{0:T(1024)} %param.23) | copy-start | bytes 24580
  6.5 7.9 %copy-start.2 = (f32[16,2,128,128]{3,2,1,0:T(8,128)S(1)}, f32[16,2,128,128]{3,2,1,0:T(8,128)}, u32[]{:S(2)}) copy-start(f32[16,2,128,128]{3,2,1,0:T(8,128)} %param.22) | copy-start | bytes 6291460
  12.4 4.9 %copy-start.7 = (s32[16,6]{0,1:T(8,128)S(1)}, s32[16,6]{0,1:T(8,128)}, u32[]{:S(2)}) copy-start(s32[16,6]{0,1:T(8,128)} %param.33) | copy-start | bytes 1156
  14.5 11.3 %copy-start.9 = (f32[2048]{0:T(1024)S(1)}, f32[2048]{0:T(1024)}, u32[]{:S(2)}) copy-start(f32[2048]{0:T(1024)} %param.28) | copy-start | bytes 24580
  18.9 41.5 %copy-start.11 = (bf16[1024,256]{1,0:T(8,128)(2,1)S(1)}, bf16[1024,256]{1,0:T(8,128)(2,1)}, u32[]{:S(2)}) copy-start(bf16[1024,256]{1,0:T(8,128)(2,1)} %param.31) | copy-start | bytes 1572868
  27.0 59.8 %all-to-all-start = ((bf16[16,12,1024]{2,1,0:T(8,128)(2,1)}), bf16[16,12,1024]{2,1,0:T(8,128)(2,1)S(1)}, u32[]{:S(2)}, u32[]{:S(2)}) async-start(bf16[16,12,1024]{2,1,0:T(8,128)(2,1)} %reshape.155), calls=%async_computation | async-start | bytes 1048576 | tf_op jit(solution)/shard_map/all_to_all | solution.py:106
  33.5 52.0 %copy-start.4 = (bf16[256,1024]{1,0:T(8,128)(2,1)S(1)}, bf16[256,1024]{1,0:T(8,128)(2,1)}, u32[]{:S(2)}) copy-start(bf16[256,1024]{1,0:T(8,128)(2,1)} %param.32) | copy-start | bytes 1572868
  33.5 51.0 %all-reduce.2.cloned.1.call-start = ((), (), s32[]{:S(2)}) async-start(), calls=%async_computation.4 | async-start | bytes 524288 | tf_op jit(solution)/shard_map/psum | solution.py:137
  62.6 85.8 %reduce-scatter.2.cloned.1.call-start = ((), (), s32[]{:S(2)}) async-start(), calls=%async_computation.5 | async-start | bytes 1114112 | tf_op jit(solution)/shard_map/reduce_scatter | solution.py:143
  85.5 12.6 %copy-start.3 = (bf16[1,2048,256]{2,1,0:T(8,128)(2,1)S(1)}, bf16[1,2048,256]{2,1,0:T(8,128)(2,1)}, u32[]{:S(2)}) copy-start(bf16[1,2048,256]{2,1,0:T(8,128)(2,1)} %param.35) | copy-start | bytes 3145732
  100.9 19.0 %copy-start.10 = (bf16[2048]{0:T(1024)(128)(2,1)S(1)}, bf16[2048]{0:T(1024)(128)(2,1)}, u32[]{:S(2)}) copy-start(bf16[2048]{0:T(1024)(128)(2,1)} %param.29) | copy-start | bytes 12292
  100.9 19.0 %copy-start.8 = (f32[16,6]{0,1:T(8,128)S(1)}, f32[16,6]{0,1:T(8,128)}, u32[]{:S(2)}) copy-start(f32[16,6]{0,1:T(8,128)} %param.34) | copy-start | bytes 1156
  113.0 35.5 %copy-start.5 = (f32[16,2048]{1,0:T(8,128)S(1)}, f32[16,2048]{1,0:T(8,128)}, u32[]{:S(2)}) copy-start(f32[16,2048]{1,0:T(8,128)} %get-tuple-element.6) | copy-start | bytes 393220
  114.2 21.1 %all-to-all-start.2 = ((bf16[16,12,1024]{2,1,0:T(8,128)(2,1)}), bf16[16,12,1024]{2,1,0:T(8,128)(2,1)S(1)}, u32[]{:S(2)}, u32[]{:S(2)}) async-start(bf16[16,12,1024]{2,1,0:T(8,128)(2,1)} %copy.64), calls=%async_computation.2 | async-start | bytes 1048576 | tf_op jit(solution)/shard_map/all_to_all | solution.py:124
Sparse Core Ops, SparseCore 0:
  62.8 21.6 all-reduce.1
  88.1 60.3 reduce-scatter.1
